TPU v7x, 256 devices: a 2x2x32 block of a 4x8x32 slice. The times are simulated.
256 devices in a mesh: grp: 4 (over y, x), ep: 64 (over z, core).
Axes of the slice: x: 2, y: 2, z: 32, core: 2. Of those that a mesh axis runs over, the one named last changes fastest.
The devices are a block of a 4x8x32 slice.
Arguments:
- tokens: bfloat16 [256, 2048], P(('grp', 'ep')), parts along dimension 0, may hold values from -6 to 6
- cache_latent: bfloat16 [256, 3072, 512], P(('grp', 'ep')), parts along dimension 0, may hold values from -6 to 6
- cache_rope: bfloat16 [256, 32, 3072], P(('grp', 'ep')), parts along dimension 0, may hold values from -1000 to 1000
- lengths: int32 [256], P(('grp', 'ep')), parts along dimension 0, may hold values from 384 to 3072, as said below
- w_query: bfloat16 [2048, 1536], P('ep'), may hold values from -0.125 to 0.125
- w_latent: bfloat16 [2048, 512], P('ep'), may hold values from -0.125 to 0.125
- w_rope: bfloat16 [2048, 32], P('ep'), may hold values from -0.125 to 0.125
- w_absorb: bfloat16 [512, 1024], replicated, may hold values from -0.25 to 0.25
- w_value: bfloat16 [512, 1024], replicated, may hold values from -0.25 to 0.25
- w_output: bfloat16 [1024, 2048], P('ep'), may hold values from -0.1875 to 0.1875
- gain_attn: float32 [2048], replicated, may hold values from 0.1 to 1.9
- gain_latent: float32 [512], replicated, may hold values from 0.1 to 1.9
- gain_moe: float32 [2048], replicated, may hold values from 0.1 to 1.9
- routes: int32 [256, 2], P(('grp', 'ep')), parts along dimension 0, may hold values from 0 to 63, all different within a row; in each aligned block of 64 rows (0 to 63, 64 to 127, ...) at most 4 rows name the same one
- route_scores: float32 [256, 2], P(('grp', 'ep')), parts along dimension 0, may hold values from 0.2 to 1
- w_gate: bfloat16 [64, 2048, 512], P('ep'), may hold values from -0.125 to 0.125
- w_up: bfloat16 [64, 2048, 512], P('ep'), may hold values from -0.125 to 0.125
- w_down: bfloat16 [64, 512, 2048], P('ep'), may hold values from -0.25 to 0.25
Outputs:
- mixed: bfloat16 [256, 2048], P(('grp', 'ep')), parts along dimension 0
- new_latent: bfloat16 [256, 512], P(('grp', 'ep')), parts along dimension 0
- new_rope: bfloat16 [256, 32], P(('grp', 'ep')), parts along dimension 0
There are 4 independent parts, one for each index of `grp`. A program takes and returns all parts, laid end to end along the dimension named above; an argument that names none is the same for every part. Nothing has to cross between parts.
Inputs may be any that keep to these rules, and one draw needn't show every extreme that they name: `routes`: each row names 2 different experts; over one part's 64 tokens no expert is named by more than 4 rows, a bound that some block reaches. `lengths`: some sequence has all 3072 positions filled.
All inputs are finite; a program needn't handle non-finite values.
Results may differ from a plain program's by a relative error of at most 0.013.
Values may be sent and summed in bfloat16 or wider, within the bound.
A program may use at most 64 MiB of HBM per device.

v0:
```python
import functools

import jax
import jax.numpy as jnp
import numpy as np
from jax import lax
from jax.experimental import pallas as pl
from jax.experimental.pallas import tpu as pltpu
from jax.sharding import PartitionSpec as P

HEADS = 16
NOPE = 64
ROPE = 32
VDIM = 64
LATENT = 512
EPS = 1e-06
THETA = 10000.0
MESH = pl.DeviceIdType.MESH
STEPS = (1, 3, 4)
DIGITS = (
    (0, 0, 0),
    (1, 0, 0),
    (-1, 1, 0),
    (0, 1, 0),
    (0, 0, 1),
    (1, 0, 1),
    (-1, 1, 1),
    (0, 1, 1),
    (1, 1, 1),
)
PIECES = 1
RING = (2, 5)
F32 = jnp.float32
BF16 = jnp.bfloat16


def rope_tables(position, lanes):
    place = lax.rem(lax.broadcasted_iota(jnp.int32, (1, lanes), 1), ROPE // 2)
    inverse = jnp.zeros((1, lanes), F32)
    for i in range(ROPE // 2):
        inverse = jnp.where(place == i, float(np.float32(THETA ** (-2.0 * i / ROPE))), inverse)
    angle = position.astype(F32) * inverse
    return (jnp.cos(angle), jnp.sin(angle))


def farthest_first(i, n):
    half = (i + 1) // 2
    return n // 2 + half * (1 - 2 * lax.rem(i, 2))


def rotate(x, cosine, sine):
    lanes = x.shape[-1]
    place = lax.rem(lax.broadcasted_iota(jnp.int32, x.shape, 1), ROPE)
    ahead = pltpu.roll(x, lanes - ROPE // 2, 1)
    behind = pltpu.roll(x, ROPE // 2, 1)
    return jnp.where(place < ROPE // 2, x * cosine - ahead * sine, x * cosine + behind * sine)


def dot(a, b):
    return jnp.dot(a, b, preferred_element_type=F32)


def dot_nt(a, b):
    return lax.dot_general(a, b, (((1,), (1,)), ((), ())), preferred_element_type=F32)


def kernel(
    nz,
    length_ref,
    routes_ref,
    scores_ref,
    tokens_hbm,
    cache_hbm,
    rope_hbm,
    wq_hbm,
    wl_hbm,
    wr_hbm,
    wa_hbm,
    wv_hbm,
    wo_hbm,
    gain_attn_hbm,
    gain_latent_hbm,
    gain_moe_hbm,
    wg_hbm,
    wu_hbm,
    wd_hbm,
    mixed_ref,
    new_latent_ref,
    new_rope_ref,
    tokens_v,
    gain_attn_v,
    gain_latent_v,
    gain_moe_v,
    wt_v,
    cache_v,
    rope_v,
    wa_v,
    wv_v,
    wq_v,
    wl_v,
    wr_v,
    wo_v,
    wg_v,
    wu_v,
    wd_v,
    p1_send,
    p1_recv,
    hop_send,
    hop_recv,
    wt_recv,
    p2_send,
    p2_recv,
    v_send,
    v_recv,
    o_send,
    o_recv,
    p3_send,
    p3_recv,
    x3,
    c4,
    p4_send,
    p4_recv,
    local_sem,
    send16,
    send32,
    sendw,
    send_hop,
    recv_hop,
    wt_sem,
    p2_sem,
    p3_sem,
    p4_sem,
    w_send,
    w_recv,
    e_send,
    e_recv,
    right_send,
    right_recv,
    left_send,
    left_recv,
    twin_send,
    twin_recv,
    quad_send,
    v_sem,
    o_sem,
):
    g = lax.axis_index("grp")
    q = lax.rem(g, 2)
    e = lax.axis_index("ep")
    z = e // 2
    c = lax.rem(e, 2)
    m = z // 2
    p = lax.rem(z, 2)
    nm = nz // 2
    q_width = wq_hbm.shape[1]
    lat = wl_hbm.shape[1]
    ropes = wr_hbm.shape[1]
    fper = wq_hbm.shape[0]
    feats = 4 * fper
    d_model = tokens_hbm.shape[1]
    half = d_model // 2
    cache = cache_v.shape[0]

    def dev(zz, cc):
        return (g, zz * 2 + cc)

    beside = z + 1 - 2 * p
    right = lax.rem(z + 1, nz)
    left = lax.rem(z + nz - 1, nz)

    def remote(src, dst, send, recv, to):
        return pltpu.make_async_remote_copy(
            src_ref=src, dst_ref=dst, send_sem=send, recv_sem=recv, device_id=to, device_id_type=MESH
        )

    barrier = pltpu.get_barrier_semaphore()

    near = [dev(lax.rem(z + nz + k, nz), c) for k in (1, -1, 2, -2, 4, -4)]
    near += [dev(z, 1 - c), dev(beside, 1 - c), (g + 1 - 2 * q, e)]
    for device in near:
        pl.semaphore_signal(barrier, inc=1, device_id=device, device_id_type=MESH)

    block = 2 * p + c
    rows = pl.ds(pl.multiple_of(block * fper, fper), fper)
    loads = [
        (tokens_hbm, tokens_v),
        (gain_attn_hbm, gain_attn_v),
        (wq_hbm, wq_v.at[rows]),
        (wl_hbm, wl_v.at[rows]),
        (wr_hbm, wr_v.at[rows]),
        (gain_latent_hbm, gain_latent_v),
        (gain_moe_hbm, gain_moe_v),
        (wo_hbm, wo_v.at[m]),
        (wa_hbm, wa_v),
        (cache_hbm.at[0], cache_v),
        (rope_hbm.at[0], rope_v),
        (wv_hbm, wv_v),
        (wg_hbm.at[0], wg_v.at[c]),
        (wu_hbm.at[0], wu_v.at[c]),
        (wd_hbm.at[0], wd_v.at[c]),
    ]
    local = [pltpu.make_async_copy(a, b, local_sem.at[i]) for i, (a, b) in enumerate(loads)]
    for copy in local:
        copy.start()

    local[0].wait()
    local[1].wait()
    tokens = tokens_v[...].astype(F32)
    normed = tokens * lax.rsqrt(jnp.mean(tokens * tokens, axis=-1, keepdims=True) + EPS) * gain_attn_v[...]
    normed = normed.astype(BF16).astype(F32)
    blocks = [normed[:, i * feats : (i + 1) * feats] for i in range(nm)]
    for i in range(nm):
        p1_send[i] = blocks[i]
    p1_recv[m] = p1_send[m]
    lane = lax.broadcasted_iota(jnp.int32, wt_v.shape, 1)
    first = jnp.full(wt_v.shape, scores_ref[0, 0], F32)
    second = jnp.full(wt_v.shape, scores_ref[0, 1], F32)
    both = first + second
    wt_v[...] = jnp.where(lane == routes_ref[0, 0], first / both, 0.0) + jnp.where(
        lane == routes_ref[0, 1], second / both, 0.0
    )
    wt_recv[z] = wt_v[...]
    cosine, sine = rope_tables(length_ref[0], HEADS * ROPE)
    p2_send[...] = jnp.zeros_like(p2_send)

    pl.semaphore_wait(barrier, len(near))

    w_pairs = ((wq_hbm, wq_v), (wl_hbm, wl_v), (wr_hbm, wr_v))
    w_targets = (dev(beside, c), dev(z, 1 - c))
    across = 2 * (1 - p) + c

    def w_copies(slot, k):
        at = pl.ds(pl.multiple_of(slot * fper, fper), fper)
        return [
            remote(
                src if k < 2 else dst.at[at],
                dst.at[at],
                w_send.at[3 * k + j],
                w_recv.at[3 * slot + j],
                w_targets[min(k, 1)],
            )
            for j, (src, dst) in enumerate(w_pairs)
        ]

    piece = half // PIECES

    def member(k):
        return lax.rem(m + nm + k, nm)

    def to_class(k):
        return dev(2 * member(k) + p, c)

    def lanes_of(which, k):
        return pl.ds(pl.multiple_of(which * half + k * piece, piece), piece)

    def wo_piece(mm, k):
        return wo_v.at[mm, :, lanes_of(q, k)]

    def to_twin(mm, k, which):
        part = wo_v.at[mm, :, lanes_of(which, k)]
        i = mm * PIECES + k
        return remote(part, part, twin_send.at[i], twin_recv.at[i], (g + 1 - 2 * q, e))

    def to_right(mm, s, k, src=None):
        i = s * PIECES + k
        dst = wo_piece(mm, k)
        return remote(dst if src is None else src, dst, right_send.at[i], right_recv.at[i], to_class(1))

    def to_left(mm, s, k, src=None):
        i = s * PIECES + k
        dst = wo_piece(mm, k)
        return remote(dst if src is None else src, dst, left_send.at[i], left_recv.at[i], to_class(-1))

    def ring_start():
        for k in range(PIECES):
            own = wo_hbm.at[:, lanes_of(q, k)]
            to_right(m, 0, k, own).start()
            to_left(m, 0, k, own).start()

    def ring_step(s, leftward, pass_right, pass_left):
        from_left = member(-s)
        from_right = member(s)
        for k in range(PIECES):
            to_right(from_left, s - 1, k).wait_recv()
            if pass_right:
                to_right(from_left, s, k).start()
            to_twin(from_left, k, q).start()
            if leftward:
                to_left(from_right, s - 1, k).wait_recv()
                if pass_left:
                    to_left(from_right, s, k).start()
                to_twin(from_right, k, q).start()

    def ring(first, last):
        for s in range(first, last + 1):
            ring_step(s, s < nm // 2, s < nm // 2, s < nm // 2 - 1)

    e_pairs = ((wg_hbm, wg_v), (wu_hbm, wu_v), (wd_hbm, wd_v))

    def e_copies(slot):
        return [
            remote(src.at[0], dst.at[slot], e_send.at[j], e_recv.at[j], dev(z, 1 - c))
            for j, (src, dst) in enumerate(e_pairs)
        ]

    digits = {o: DIGITS[abs(o)] if o >= 0 else tuple(-x for x in DIGITS[-o]) for o in range(1 - nm // 2, nm // 2 + 1)}
    place = {}
    for r in range(len(STEPS)):
        for sign in (1, -1):
            at = [o for o in digits if digits[o][r] == sign]
            for i, o in enumerate(at):
                place[o, r] = i

    def p1_round(r, sign):
        count = sum(1 for o in digits if digits[o][r] == sign)
        to = 2 * member(sign * STEPS[r]) + p
        i = 2 * r + (sign < 0)
        part = pl.ds(0, count)
        return remote(hop_send.at[i, part], hop_recv.at[i, part], send_hop.at[i], recv_hop.at[i], dev(to, c))

    def last_hop(o, r):
        for earlier in range(r - 1, -1, -1):
            if digits[o][earlier]:
                return earlier
        return None

    def p1_start(r):
        for o in digits:
            if digits[o][r]:
                held = last_hop(o, r)
                if held is None:
                    block_o = p1_send[member(o)]
                else:
                    block_o = hop_recv[2 * held + (digits[o][held] < 0), place[o, held]]
                hop_send[2 * r + (digits[o][r] < 0), place[o, r]] = block_o
        p1_round(r, 1).start()
        p1_round(r, -1).start()

    def p1_wait(r):
        p1_round(r, 1).wait_recv()
        p1_round(r, -1).wait_recv()

    p1_start(0)
    for k in range(2):
        for copy in w_copies(block, k):
            copy.start()
    ring_start()
    for copy in e_copies(c):
        copy.start()
    p1_wait(0)
    p1_start(1)
    for here, there in zip(w_copies(across, 0), w_copies(across, 2)):
        here.wait_recv()
        there.start()
    ring(1, RING[0])
    p1_wait(1)
    p1_start(2)
    ring(RING[0] + 1, RING[1])

    for copy in local[2:5]:
        copy.wait()
    for slot in (2 * p + 1 - c, 2 * (1 - p) + 1 - c):
        for copy in w_copies(slot, 1):
            copy.wait_recv()
    p1_wait(2)
    for o in digits:
        if o:
            held = last_hop(o, len(STEPS))
            p1_recv[member(-o)] = hop_recv[2 * held + (digits[o][held] < 0), place[o, held]]

    x1 = p1_recv[:, 0, :].astype(BF16)
    part_q = dot(x1, wq_v[...])
    part_l = dot(x1, wl_v[...])
    part_r = dot(x1, wr_v[...])
    for i in range(nm):
        p2_send[i, :, 0:q_width] = part_q[i : i + 1, :]
        p2_send[i, :, q_width : q_width + lat] = part_l[i : i + 1, :]
        p2_send[i, :, q_width + lat : q_width + lat + ropes] = part_r[i : i + 1, :]

    def p2_copy(to, slot, d):
        return remote(p2_send.at[to], p2_recv.at[slot], send16.at[d], p2_sem.at[slot], dev(2 * to + p, c))

    def p2_start(i, _):
        d = farthest_first(i, nm)
        p2_copy(lax.rem(m + d, nm), m, d).start()
        return 0

    lax.fori_loop(0, nm - 1, p2_start, 0)

    ring(RING[1] + 1, nm // 2)

    def p2_wait(i, acc):
        d = nm - 1 - i
        src = lax.rem(m + nm - d, nm)
        p2_copy(m, src, d).wait_recv()
        return acc + p2_recv[src]

    summed = lax.fori_loop(0, nm - 1, p2_wait, p2_send[m])

    for copy in local[5:7]:
        copy.wait()
    query = summed[:, :q_width].astype(BF16).astype(F32)
    latent_raw = summed[:, q_width : q_width + lat].astype(BF16).astype(F32)
    rope_raw = summed[:, q_width + lat :].astype(BF16).astype(F32)
    new_latent = (
        latent_raw
        * lax.rsqrt(jnp.mean(latent_raw * latent_raw, axis=-1, keepdims=True) + EPS)
        * gain_latent_v[...]
    ).astype(BF16)
    new_rope = rotate(rope_raw, cosine[:, : rope_raw.shape[1]], sine[:, : rope_raw.shape[1]]).astype(BF16)
    new_latent_ref[...] = new_latent
    new_rope_ref[...] = new_rope[:, :ropes]

    size = NOPE + ROPE
    q_nope = jnp.concatenate([query[:, h * size : h * size + NOPE] for h in range(HEADS)], axis=1)
    q_rope = jnp.concatenate([query[:, h * size + NOPE : (h + 1) * size] for h in range(HEADS)], axis=1)
    q_rope = rotate(q_rope, cosine, sine).astype(BF16).astype(F32)

    def by_head(row, width):
        shape = (HEADS, row.shape[1])
        own = lax.broadcasted_iota(jnp.int32, shape, 1) // width == lax.broadcasted_iota(jnp.int32, shape, 0)
        return jnp.where(own, jnp.broadcast_to(row, shape), 0.0)

    fold_shape = (HEADS * ROPE, ROPE)
    fold = (
        lax.rem(lax.broadcasted_iota(jnp.int32, fold_shape, 0), ROPE)
        == lax.broadcasted_iota(jnp.int32, fold_shape, 1)
    ).astype(F32).astype(BF16)
    q_pe = dot(by_head(q_rope, ROPE).astype(BF16), fold).astype(BF16)
    local[8].wait()
    q_abs = dot_nt(by_head(q_nope, NOPE).astype(BF16), wa_v[...]).astype(BF16)

    local[9].wait()
    local[10].wait()
    scale = (NOPE + ROPE) ** (-0.5)
    past = (dot_nt(q_abs, cache_v[...]) + dot(q_pe, rope_v[...])) * scale
    fresh = (
        jnp.sum(q_abs.astype(F32) * new_latent.astype(F32), axis=-1, keepdims=True)
        + jnp.sum(q_pe.astype(F32) * new_rope[:, :ropes].astype(F32), axis=-1, keepdims=True)
    ) * scale
    valid = lax.broadcasted_iota(jnp.int32, past.shape, 1) < length_ref[0]
    top = jnp.maximum(jnp.max(jnp.where(valid, past, -jnp.inf), axis=-1, keepdims=True), fresh)
    e_past = jnp.where(valid, jnp.exp(past - top), 0.0)
    e_new = jnp.exp(fresh - top)
    total = jnp.sum(e_past, axis=-1, keepdims=True) + e_new
    p_past = (e_past / total).astype(BF16)
    p_new = (e_new / total).astype(BF16).astype(F32)
    attended = (dot(p_past, cache_v[...]) + p_new * new_latent.astype(F32)).astype(BF16)
    local[11].wait()
    crossed = dot(attended, wv_v[...])
    own_head = (
        lax.broadcasted_iota(jnp.int32, crossed.shape, 1) // VDIM
        == lax.broadcasted_iota(jnp.int32, crossed.shape, 0)
    )
    values = jnp.sum(jnp.where(own_head, crossed, 0.0), axis=0, keepdims=True).astype(BF16)

    def beside_me(slot):
        return dev(z - p + slot // 2, lax.rem(slot, 2))

    def v_copy(slot, k):
        return remote(v_send, v_recv.at[slot], quad_send.at[k], v_sem.at[slot], beside_me(lax.rem(block + k, 4)))

    def o_copy(to, slot, k):
        return remote(o_send.at[to], o_recv.at[slot], quad_send.at[3 + k], o_sem.at[slot], beside_me(to))

    v_send[...] = values.astype(F32)
    for k in range(1, 4):
        v_copy(block, k).start()
    v_recv[block] = v_send[...]

    vals, own_rows = HEADS * VDIM, nm * wo_hbm.shape[0]
    vper = wo_hbm.shape[0]
    at = lax.broadcasted_iota(jnp.int32, (vals, own_rows), 0)
    row = lax.broadcasted_iota(jnp.int32, (vals, own_rows), 1)
    pick = (at == (4 * (row // vper) + block) * vper + lax.rem(row, vper)).astype(F32).astype(BF16)
    local[7].wait()
    for i in range(1, nm):
        for k in range(PIECES):
            to_twin(member(i), k, 1 - q).wait_recv()
    for k in range(1, 4):
        v_copy(lax.rem(block + k, 4), k).wait_recv()
    picked = dot(v_recv[:, 0, :].astype(BF16), pick).astype(BF16)
    part_o = dot(picked, wo_v[...].reshape(own_rows, d_model))
    for i in range(4):
        o_send[i] = part_o[i : i + 1, :]
    for k in range(1, 4):
        o_copy(lax.rem(block + k, 4), block, k).start()

    def wt_copy(to, slot, d):
        return remote(wt_v, wt_recv.at[slot], sendw.at[d], wt_sem.at[slot], dev(to, c))

    def wt_start(i, _):
        d = farthest_first(i, nz)
        wt_copy(lax.rem(z + d, nz), z, d).start()
        return 0

    lax.fori_loop(0, nz - 1, wt_start, 0)

    attn_out = o_send[block]
    for k in range(1, 4):
        slot = lax.rem(block + k, 4)
        o_copy(block, slot, k).wait_recv()
        attn_out = attn_out + o_recv[slot]
    resid = (tokens + attn_out).astype(BF16).astype(F32)
    moe_in = resid * lax.rsqrt(jnp.mean(resid * resid, axis=-1, keepdims=True) + EPS) * gain_moe_v[...]
    moe_in = moe_in.astype(BF16).astype(F32)
    p3_send[...] = jnp.concatenate([moe_in[:, :half], moe_in[:, half:]], axis=0).astype(BF16)

    def p3_copy(to, slot, d):
        return remote(p3_send, p3_recv.at[slot], send32.at[d], p3_sem.at[slot], dev(to, c))

    def p3_start(i, _):
        d = farthest_first(i, nz)
        p3_copy(lax.rem(z + d, nz), z, d).start()
        return 0

    lax.fori_loop(0, nz - 1, p3_start, 0)
    x3[pl.ds(z, 1), :] = moe_in

    for copy in local[12:15]:
        copy.wait()
    for copy in e_copies(1 - c):
        copy.wait_recv()

    def wt_wait(i, _):
        d = i + 1
        wt_copy(z, lax.rem(z + nz - d, nz), d).wait()
        return 0

    lax.fori_loop(0, nz - 1, wt_wait, 0)

    def p3_wait(i, _):
        near = i // 2 + 1
        src = lax.rem(z + nz + near * (1 - 2 * lax.rem(i, 2)), nz)
        p3_copy(z, src, 0).wait_recv()
        row = p3_recv[src].astype(F32)
        x3[pl.ds(src, 1), 0:half] = row[0:1]
        x3[pl.ds(src, 1), half:d_model] = row[1:2]
        return 0

    lax.fori_loop(0, nz - 1, p3_wait, 0)

    def p3_sent(d, _):
        p3_copy(z, z, d).wait_send()
        return 0

    lax.fori_loop(1, nz, p3_sent, 0)

    rows3 = x3[...].astype(BF16)
    shares = wt_recv[:, 0, :]
    expert = lax.broadcasted_iota(jnp.int32, shares.shape, 1)
    outs = []
    for s in range(2):
        share = jnp.sum(jnp.where(expert == 2 * z + s, shares, 0.0), axis=1, keepdims=True)
        gate = dot(rows3, wg_v[s])
        upper = dot(rows3, wu_v[s])
        hidden = (jax.nn.silu(gate) * upper).astype(BF16)
        result = dot(hidden, wd_v[s]).astype(BF16).astype(F32)
        outs.append(share * result)
    c4[...] = outs[0] + outs[1]

    def p4_copy(to, slot, d):
        return remote(p4_send.at[to], p4_recv.at[slot], send32.at[d], p4_sem.at[slot], dev(to, c))

    def p4_start(i, _):
        d = farthest_first(i, nz)
        to = lax.rem(z + d, nz)
        row = c4[pl.ds(to, 1), :]
        p4_send[to] = jnp.concatenate([row[:, :half], row[:, half:]], axis=0).astype(BF16)
        p4_copy(to, z, d).start()
        return 0

    lax.fori_loop(0, nz - 1, p4_start, 0)
    mine = c4[pl.ds(z, 1), :]

    def p4_wait(i, acc):
        near = i // 2 + 1
        src = lax.rem(z + nz + near * (1 - 2 * lax.rem(i, 2)), nz)
        p4_copy(z, src, 0).wait_recv()
        return acc + p4_recv[src].astype(F32)

    acc = lax.fori_loop(
        0, nz - 1, p4_wait, jnp.concatenate([mine[:, :half], mine[:, half:]], axis=0)
    )
    mixed_ref[:, :half] = (resid[:, :half] + acc[0:1]).astype(BF16)
    mixed_ref[:, half:] = (resid[:, half:] + acc[1:2]).astype(BF16)

    def p4_sent(d, _):
        p4_copy(z, z, d).wait_send()
        return 0

    lax.fori_loop(1, nz, p4_sent, 0)

    def p2_sent(d, _):
        p2_copy(m, m, d).wait_send()
        return 0

    lax.fori_loop(1, nm, p2_sent, 0)
    for k in range(2):
        for copy in w_copies(block, k):
            copy.wait_send()
    for copy in w_copies(across, 2):
        copy.wait_send()
    for copy in e_copies(c):
        copy.wait_send()

    for i in range(nm // 2):
        for k in range(PIECES):
            to_right(m, i, k).wait_send()
            if i < nm // 2 - 1:
                to_left(m, i, k).wait_send()
    for i in range(1, nm):
        for k in range(PIECES):
            to_twin(member(i), k, q).wait_send()
    for k in range(1, 4):
        v_copy(block, k).wait_send()
        o_copy(block, block, k).wait_send()
    for r in range(len(STEPS)):
        p1_round(r, 1).wait_send()
        p1_round(r, -1).wait_send()


def hand_over(a, b, c, x, y, w):
    x[...] = a[...]
    y[...] = b[...]
    w[...] = c[...]


def solution(mesh):
    n = mesh.shape["ep"]
    nz = n // 2
    nm = nz // 2

    def body(
        tokens,
        cache_latent,
        cache_rope,
        lengths,
        w_query,
        w_latent,
        w_rope,
        w_absorb,
        w_value,
        w_output,
        gain_attn,
        gain_latent,
        gain_moe,
        routes,
        route_scores,
        w_gate,
        w_up,
        w_down,
    ):
        d = tokens.shape[1]
        lanes = max(128, n)
        fper = w_query.shape[0]
        feats = 4 * fper
        width = w_query.shape[1] + w_latent.shape[1]
        wide = width + 128
        ff = w_gate.shape[2]
        inputs = (
            lengths,
            routes,
            route_scores,
            tokens,
            cache_latent,
            cache_rope,
            w_query,
            w_latent,
            w_rope,
            w_absorb,
            w_value,
            w_output,
            gain_attn[None, :],
            gain_latent[None, :],
            gain_moe[None, :],
            w_gate,
            w_up,
            w_down,
        )
        dma = pltpu.SemaphoreType.DMA
        outs = pl.pallas_call(
            functools.partial(kernel, nz),
            out_shape=(
                jax.ShapeDtypeStruct((1, d), BF16),
                jax.ShapeDtypeStruct((1, LATENT), BF16),
                jax.ShapeDtypeStruct((1, ROPE), BF16),
            ),
            in_specs=[pl.BlockSpec(memory_space=pltpu.SMEM)] * 3
            + [pl.BlockSpec(memory_space=pl.ANY)] * (len(inputs) - 3),
            out_specs=(pl.BlockSpec(memory_space=pltpu.VMEM),) * 3,
            scratch_shapes=[
                pltpu.VMEM((1, d), BF16),
                pltpu.VMEM((1, d), F32),
                pltpu.VMEM((1, LATENT), F32),
                pltpu.VMEM((1, d), F32),
                pltpu.VMEM((1, lanes), F32),
                pltpu.VMEM(cache_latent.shape[1:], BF16),
                pltpu.VMEM(cache_rope.shape[1:], BF16),
                pltpu.VMEM(w_absorb.shape, BF16),
                pltpu.VMEM(w_value.shape, BF16),
                pltpu.VMEM((feats, w_query.shape[1]), BF16),
                pltpu.VMEM((feats, w_latent.shape[1]), BF16),
                pltpu.VMEM((feats, w_rope.shape[1]), BF16),
                pltpu.VMEM((nm,) + w_output.shape, BF16),
                pltpu.VMEM((2, d, ff), BF16),
                pltpu.VMEM((2, d, ff), BF16),
                pltpu.VMEM((2, ff, d), BF16),
                pltpu.VMEM((nm, 1, feats), F32),
                pltpu.VMEM((nm, 1, feats), F32),
                pltpu.VMEM((6, 5, 1, feats), F32),
                pltpu.VMEM((6, 5, 1, feats), F32),
                pltpu.VMEM((nz, 1, lanes), F32),
                pltpu.VMEM((nm, 1, wide), F32),
                pltpu.VMEM((nm, 1, wide), F32),
                pltpu.VMEM((1, HEADS * VDIM), F32),
                pltpu.VMEM((4, 1, HEADS * VDIM), F32),
                pltpu.VMEM((4, 1, d), F32),
                pltpu.VMEM((4, 1, d), F32),
                pltpu.VMEM((2, d // 2), BF16),
                pltpu.VMEM((nz, 2, d // 2), BF16),
                pltpu.VMEM((nz, d), F32),
                pltpu.VMEM((nz, d), F32),
                pltpu.VMEM((nz, 2, d // 2), BF16),
                pltpu.VMEM((nz, 2, d // 2), BF16),
                dma((15,)),
                dma((nm,)),
                dma((nz,)),
                dma((nz,)),
                dma((6,)),
                dma((6,)),
                dma((nz,)),
                dma((nm,)),
                dma((nz,)),
                dma((nz,)),
                dma((9,)),
                dma((12,)),
                dma((3,)),
                dma((3,)),
                dma((nm // 2 * PIECES,)),
                dma((nm // 2 * PIECES,)),
                dma((nm // 2 * PIECES,)),
                dma((nm // 2 * PIECES,)),
                dma((nm * PIECES,)),
                dma((nm * PIECES,)),
                dma((7,)),
                dma((4,)),
                dma((4,)),
            ],
            compiler_params=pltpu.CompilerParams(
                collective_id=0, has_side_effects=True, vmem_limit_bytes=60 * 1024 * 1024
            ),
        )(*inputs)
        return pl.pallas_call(
            hand_over,
            out_shape=tuple(jax.ShapeDtypeStruct(o.shape, o.dtype) for o in outs),
            in_specs=[pl.BlockSpec(memory_space=pltpu.VMEM)] * 3,
            out_specs=(pl.BlockSpec(memory_space=pltpu.VMEM),) * 3,
        )(*outs)

    rows = P(("grp", "ep"), None)
    cached = P(("grp", "ep"), None, None)
    held = P("ep", None)
    experts = P("ep", None, None)
    return jax.shard_map(
        body,
        mesh=mesh,
        in_specs=(
            rows,
            cached,
            cached,
            P(("grp", "ep")),
            held,
            held,
            held,
            P(),
            P(),
            held,
            P(),
            P(),
            P(),
            rows,
            rows,
            experts,
            experts,
            experts,
        ),
        out_specs=(rows, rows, rows),
        check_vma=False,
    )
```

profile of v0, /device:TPU:46, one launch (start us, length us, event | category | flops | bytes accessed | tf_op | source)
XLA Modules:
  0.0 116.9 jit_solution(6163856294882591339)
XLA Ops:
  1.3 114.3 %shard_map.193 = (bf16[1,2048]{1,0:T(2,128)(2,1)}, bf16[1,512]{1,0:T(2,128)(2,1)}, bf16[1,32]{1,0:T(2,128)(2,1)}) custom-call(s32[1]{0:T(128)S(6)} %copy.21.length_ref, s32[1,2]{1,0:T(1,128)} %routes_ref.1, f32[1,2]{1,0:T(1,128)} %scores_ref.1, bf16[1,2048]{1,0:T(2,128)(2,1)} %tokens_hbm.1, bf16[1,3072,512]{2,1,0:T(8,128)(2,1)} %cache_hbm.1, ...), custom_call_target="tpu_custom_call" | custom-call | tf_op jit(solution)/shard_map/pallas_call | solution.py:682
  115.6 1.3 %shard_map.194 = (bf16[1,2048]{1,0:T(2,128)(2,1)}, bf16[1,512]{1,0:T(2,128)(2,1)}, bf16[1,32]{1,0:T(2,128)(2,1)}) custom-call(bf16[1,2048]{1,0:T(2,128)(2,1)} %get-tuple-element.6.a, bf16[1,512]{1,0:T(2,128)(2,1)} %get-tuple-element.7.b, bf16[1,32]{1,0:T(2,128)(2,1)} %get-tuple-element.8.c), custom_call_target="tpu_custom_call" | custom-call | tf_op jit(solution)/shard_map/pallas_call | solution.py:754
where the time goes:
time: 117 us
  Pallas kernels  116 us (99%)
  between operations  1.29 us (1%)
    pallas_call x1, Pallas kernels, body(): pl.pallas_call(functools.partial(kernel, nz), out_shape=(jax.ShapeDtypeSt...  114 us

commit v1 on v0

--- a/solution.py
+++ b/solution.py
@@ -29,7 +29,7 @@
     (1, 1, 1),
 )
 PIECES = 1
-RING = (2, 5)
+RING = (2, 4)
 F32 = jnp.float32
 BF16 = jnp.bfloat16
 
@@ -110,6 +110,8 @@
     wt_recv,
     p2_send,
     p2_recv,
+    p2r_send,
+    p2r_recv,
     v_send,
     v_recv,
     o_send,
@@ -122,12 +124,14 @@
     p4_recv,
     local_sem,
     send16,
+    send16r,
     send32,
     sendw,
     send_hop,
     recv_hop,
     wt_sem,
     p2_sem,
+    p2r_sem,
     p3_sem,
     p4_sem,
     w_send,
@@ -152,8 +156,6 @@
     m = z // 2
     p = lax.rem(z, 2)
     nm = nz // 2
-    q_width = wq_hbm.shape[1]
-    lat = wl_hbm.shape[1]
     ropes = wr_hbm.shape[1]
     fper = wq_hbm.shape[0]
     feats = 4 * fper
@@ -221,7 +223,7 @@
     )
     wt_recv[z] = wt_v[...]
     cosine, sine = rope_tables(length_ref[0], HEADS * ROPE)
-    p2_send[...] = jnp.zeros_like(p2_send)
+    p2r_send[...] = jnp.zeros_like(p2r_send)
 
     pl.semaphore_wait(barrier, len(near))
 
@@ -372,36 +374,51 @@
     part_q = dot(x1, wq_v[...])
     part_l = dot(x1, wl_v[...])
     part_r = dot(x1, wr_v[...])
+    size = NOPE + ROPE
+    nope, turned = HEADS * NOPE, HEADS * ROPE
+    part_n = jnp.concatenate([part_q[:, h * size : h * size + NOPE] for h in range(HEADS)], axis=1)
+    part_p = jnp.concatenate([part_q[:, h * size + NOPE : (h + 1) * size] for h in range(HEADS)], axis=1)
+    plain = jnp.concatenate([part_n, part_l], axis=1)
+    fold2 = plain.shape[1] // 2
     for i in range(nm):
-        p2_send[i, :, 0:q_width] = part_q[i : i + 1, :]
-        p2_send[i, :, q_width : q_width + lat] = part_l[i : i + 1, :]
-        p2_send[i, :, q_width + lat : q_width + lat + ropes] = part_r[i : i + 1, :]
+        row = plain[i : i + 1, :]
+        p2_send[i] = jnp.concatenate([row[:, :fold2], row[:, fold2:]], axis=0).astype(BF16)
+        p2r_send[i, :, 0:turned] = part_p[i : i + 1, :]
+        p2r_send[i, :, turned : turned + ropes] = part_r[i : i + 1, :]
 
     def p2_copy(to, slot, d):
         return remote(p2_send.at[to], p2_recv.at[slot], send16.at[d], p2_sem.at[slot], dev(2 * to + p, c))
 
+    def p2r_copy(to, slot, d):
+        return remote(p2r_send.at[to], p2r_recv.at[slot], send16r.at[d], p2r_sem.at[slot], dev(2 * to + p, c))
+
     def p2_start(i, _):
         d = farthest_first(i, nm)
-        p2_copy(lax.rem(m + d, nm), m, d).start()
+        to = lax.rem(m + d, nm)
+        p2r_copy(to, m, d).start()
+        p2_copy(to, m, d).start()
         return 0
 
     lax.fori_loop(0, nm - 1, p2_start, 0)
 
-    ring(RING[1] + 1, nm // 2)
+    ring(RING[1] + 1, nm // 2 - 1)
 
     def p2_wait(i, acc):
         d = nm - 1 - i
         src = lax.rem(m + nm - d, nm)
+        p2r_copy(m, src, d).wait_recv()
         p2_copy(m, src, d).wait_recv()
-        return acc + p2_recv[src]
-
-    summed = lax.fori_loop(0, nm - 1, p2_wait, p2_send[m])
+        return (acc[0] + p2_recv[src].astype(F32), acc[1] + p2r_recv[src])
+
+    folded, turns = lax.fori_loop(0, nm - 1, p2_wait, (p2_send[m].astype(F32), p2r_send[m]))
+    summed = jnp.concatenate([folded[0:1], folded[1:2]], axis=1)
 
     for copy in local[5:7]:
         copy.wait()
-    query = summed[:, :q_width].astype(BF16).astype(F32)
-    latent_raw = summed[:, q_width : q_width + lat].astype(BF16).astype(F32)
-    rope_raw = summed[:, q_width + lat :].astype(BF16).astype(F32)
+    q_nope = summed[:, :nope].astype(BF16).astype(F32)
+    q_rope = turns[:, :turned].astype(BF16).astype(F32)
+    latent_raw = summed[:, nope:].astype(BF16).astype(F32)
+    rope_raw = turns[:, turned:].astype(BF16).astype(F32)
     new_latent = (
         latent_raw
         * lax.rsqrt(jnp.mean(latent_raw * latent_raw, axis=-1, keepdims=True) + EPS)
@@ -411,9 +428,6 @@
     new_latent_ref[...] = new_latent
     new_rope_ref[...] = new_rope[:, :ropes]
 
-    size = NOPE + ROPE
-    q_nope = jnp.concatenate([query[:, h * size : h * size + NOPE] for h in range(HEADS)], axis=1)
-    q_rope = jnp.concatenate([query[:, h * size + NOPE : (h + 1) * size] for h in range(HEADS)], axis=1)
     q_rope = rotate(q_rope, cosine, sine).astype(BF16).astype(F32)
 
     def by_head(row, width):
@@ -467,6 +481,7 @@
     for k in range(1, 4):
         v_copy(block, k).start()
     v_recv[block] = v_send[...]
+    ring(nm // 2, nm // 2)
 
     vals, own_rows = HEADS * VDIM, nm * wo_hbm.shape[0]
     vper = wo_hbm.shape[0]
@@ -593,6 +608,7 @@
 
     def p2_sent(d, _):
         p2_copy(m, m, d).wait_send()
+        p2r_copy(m, m, d).wait_send()
         return 0
 
     lax.fori_loop(1, nm, p2_sent, 0)
@@ -655,8 +671,8 @@
         lanes = max(128, n)
         fper = w_query.shape[0]
         feats = 4 * fper
-        width = w_query.shape[1] + w_latent.shape[1]
-        wide = width + 128
+        plain = HEADS * NOPE + w_latent.shape[1]
+        turned = HEADS * ROPE + 128
         ff = w_gate.shape[2]
         inputs = (
             lengths,
@@ -711,8 +727,10 @@
                 pltpu.VMEM((6, 5, 1, feats), F32),
                 pltpu.VMEM((6, 5, 1, feats), F32),
                 pltpu.VMEM((nz, 1, lanes), F32),
-                pltpu.VMEM((nm, 1, wide), F32),
-                pltpu.VMEM((nm, 1, wide), F32),
+                pltpu.VMEM((nm, 2, plain // 2), BF16),
+                pltpu.VMEM((nm, 2, plain // 2), BF16),
+                pltpu.VMEM((nm, 1, turned), F32),
+                pltpu.VMEM((nm, 1, turned), F32),
                 pltpu.VMEM((1, HEADS * VDIM), F32),
                 pltpu.VMEM((4, 1, HEADS * VDIM), F32),
                 pltpu.VMEM((4, 1, d), F32),
@@ -725,11 +743,13 @@
                 pltpu.VMEM((nz, 2, d // 2), BF16),
                 dma((15,)),
                 dma((nm,)),
+                dma((nm,)),
                 dma((nz,)),
                 dma((nz,)),
                 dma((6,)),
                 dma((6,)),
                 dma((nz,)),
+                dma((nm,)),
                 dma((nm,)),
                 dma((nz,)),
                 dma((nz,)),

time: 117 us -> 115 us (0.983); the launches traced: 117 us -> 113 us
  Pallas kernels: 116 us -> 112 us
    pallas_call x1, Pallas kernels: 114 us -> 110 us  [body(): pl.pallas_call(functools.partial(kernel, nz), out_shape=(jax.ShapeDtypeSt...]
where the time goes in v1:
time: 115 us; the launch traced here: 113 us
  Pallas kernels  112 us (97%)
  between operations  1.29 us (1%)
    pallas_call x1, Pallas kernels, body(): pl.pallas_call(functools.partial(kernel, nz), out_shape=(jax.ShapeDtypeSt...  110 us

profile of v1, /device:TPU:46, one launch (start us, length us, event | category | flops | bytes accessed | tf_op | source)
XLA Modules:
  0.0 113.0 jit_solution(11639770603899057776)
XLA Ops:
  1.3 110.4 %shard_map.193 = (bf16[1,2048]{1,0:T(2,128)(2,1)}, bf16[1,512]{1,0:T(2,128)(2,1)}, bf16[1,32]{1,0:T(2,128)(2,1)}) custom-call(s32[1]{0:T(128)S(6)} %copy.21.length_ref, s32[1,2]{1,0:T(1,128)} %routes_ref.1, f32[1,2]{1,0:T(1,128)} %scores_ref.1, bf16[1,2048]{1,0:T(2,128)(2,1)} %tokens_hbm.1, bf16[1,3072,512]{2,1,0:T(8,128)(2,1)} %cache_hbm.1, ...), custom_call_target="tpu_custom_call" | custom-call | tf_op jit(solution)/shard_map/pallas_call | solution.py:698
  111.7 1.3 %shard_map.194 = (bf16[1,2048]{1,0:T(2,128)(2,1)}, bf16[1,512]{1,0:T(2,128)(2,1)}, bf16[1,32]{1,0:T(2,128)(2,1)}) custom-call(bf16[1,2048]{1,0:T(2,128)(2,1)} %get-tuple-element.6.a, bf16[1,512]{1,0:T(2,128)(2,1)} %get-tuple-element.7.b, bf16[1,32]{1,0:T(2,128)(2,1)} %get-tuple-element.8.c), custom_call_target="tpu_custom_call" | custom-call | tf_op jit(solution)/shard_map/pallas_call | solution.py:774

commit v2 on v1

--- a/solution.py
+++ b/solution.py
@@ -214,17 +214,6 @@
     for i in range(nm):
         p1_send[i] = blocks[i]
     p1_recv[m] = p1_send[m]
-    lane = lax.broadcasted_iota(jnp.int32, wt_v.shape, 1)
-    first = jnp.full(wt_v.shape, scores_ref[0, 0], F32)
-    second = jnp.full(wt_v.shape, scores_ref[0, 1], F32)
-    both = first + second
-    wt_v[...] = jnp.where(lane == routes_ref[0, 0], first / both, 0.0) + jnp.where(
-        lane == routes_ref[0, 1], second / both, 0.0
-    )
-    wt_recv[z] = wt_v[...]
-    cosine, sine = rope_tables(length_ref[0], HEADS * ROPE)
-    p2r_send[...] = jnp.zeros_like(p2r_send)
-
     pl.semaphore_wait(barrier, len(near))
 
     w_pairs = ((wq_hbm, wq_v), (wl_hbm, wl_v), (wr_hbm, wr_v))
@@ -349,6 +338,16 @@
     ring_start()
     for copy in e_copies(c):
         copy.start()
+    lane = lax.broadcasted_iota(jnp.int32, wt_v.shape, 1)
+    first = jnp.full(wt_v.shape, scores_ref[0, 0], F32)
+    second = jnp.full(wt_v.shape, scores_ref[0, 1], F32)
+    both = first + second
+    wt_v[...] = jnp.where(lane == routes_ref[0, 0], first / both, 0.0) + jnp.where(
+        lane == routes_ref[0, 1], second / both, 0.0
+    )
+    wt_recv[z] = wt_v[...]
+    cosine, sine = rope_tables(length_ref[0], HEADS * ROPE)
+    p2r_send[...] = jnp.zeros_like(p2r_send)
     p1_wait(0)
     p1_start(1)
     for here, there in zip(w_copies(across, 0), w_copies(across, 2)):
@@ -401,7 +400,7 @@
 
     lax.fori_loop(0, nm - 1, p2_start, 0)
 
-    ring(RING[1] + 1, nm // 2 - 1)
+    ring(RING[1] + 1, nm // 2 - 2)
 
     def p2_wait(i, acc):
         d = nm - 1 - i
@@ -444,6 +443,7 @@
     local[8].wait()
     q_abs = dot_nt(by_head(q_nope, NOPE).astype(BF16), wa_v[...]).astype(BF16)
 
+    ring(nm // 2 - 1, nm // 2 - 1)
     local[9].wait()
     local[10].wait()
     scale = (NOPE + ROPE) ** (-0.5)

time: 115 us -> 114 us (level)
  no operation moved by 1% of the time
where the time goes in v2:
time: 114 us; the launch traced here: 112 us
  Pallas kernels  111 us (97%)
  between operations  1.29 us (1%)
    pallas_call x1, Pallas kernels, body(): pl.pallas_call(functools.partial(kernel, nz), out_shape=(jax.ShapeDtypeSt...  110 us

profile of v2, /device:TPU:46, one launch (start us, length us, event | category | flops | bytes accessed | tf_op | source)
XLA Modules:
  0.0 112.4 jit_solution(12078890761783564088)
XLA Ops:
  1.3 109.8 %shard_map.193 = (bf16[1,2048]{1,0:T(2,128)(2,1)}, bf16[1,512]{1,0:T(2,128)(2,1)}, bf16[1,32]{1,0:T(2,128)(2,1)}) custom-call(s32[1]{0:T(128)S(6)} %copy.21.length_ref, s32[1,2]{1,0:T(1,128)} %routes_ref.1, f32[1,2]{1,0:T(1,128)} %scores_ref.1, bf16[1,2048]{1,0:T(2,128)(2,1)} %tokens_hbm.1, bf16[1,3072,512]{2,1,0:T(8,128)(2,1)} %cache_hbm.1, ...), custom_call_target="tpu_custom_call" | custom-call | tf_op jit(solution)/shard_map/pallas_call | solution.py:698
  111.1 1.3 %shard_map.194 = (bf16[1,2048]{1,0:T(2,128)(2,1)}, bf16[1,512]{1,0:T(2,128)(2,1)}, bf16[1,32]{1,0:T(2,128)(2,1)}) custom-call(bf16[1,2048]{1,0:T(2,128)(2,1)} %get-tuple-element.6.a, bf16[1,512]{1,0:T(2,128)(2,1)} %get-tuple-element.7.b, bf16[1,32]{1,0:T(2,128)(2,1)} %get-tuple-element.8.c), custom_call_target="tpu_custom_call" | custom-call | tf_op jit(solution)/shard_map/pallas_call | solution.py:774
